TPU v7x, 32 devices: a whole 2x2x4 slice. The times are simulated.
32 devices in a mesh: fs: 8 (over z, core), tp: 4 (over y, x).
Axes of the slice: x: 2, y: 2, z: 4, core: 2. Of those that a mesh axis runs over, the one named last changes fastest.
Arguments:
- prompt: bfloat16 [1024, 2048], P('tp'), may hold values from -6 to 6
- norm_gain: float32 [2048], P('fs'), may hold values from 0.1 to 1.9
- gate_master: float32 [32, 2048, 512], P(None, 'fs', 'tp'), may hold values from -6 to 6
- up_master: float32 [32, 2048, 512], P(None, 'fs', 'tp'), may hold values from -6 to 6
- down_master: float32 [32, 2048, 512], P(None, 'fs', 'tp'), may hold values from -6 to 6
- group_choice: int32 [1024], P('tp'), may hold values from 0 to 3
- inner_choice: int32 [1024, 2], P('tp'), may hold values from 0 to 7, as said below
- route_weight: float32 [1024, 2], P('tp'), may hold values from 0.2 to 1
Outputs:
- gate_served: bfloat16 [2048, 16384], P(None, 'fs')
- up_served: bfloat16 [2048, 16384], P(None, 'fs')
- down_served: bfloat16 [2048, 16384], P(None, 'fs')
- mixed: bfloat16 [1024, 2048], P('tp', 'fs')
Inputs may be any that keep to these rules, and one draw needn't show every extreme that they name: `inner_choice`: the two experts of a token differ.
All inputs are finite; a program needn't handle non-finite values.
Results may differ from a plain program's by a relative error of at most 0.0081.
Values may be sent and summed in bfloat16 or wider, within the bound.
A program may use at most 128 MiB of HBM per device.

v0:
```python
import jax
import jax.numpy as jnp
from jax import lax
from jax.sharding import PartitionSpec as P

FF = 512
GROUPS = 4
EPG = 8


def flatten_rows(piece):
    count, experts, rows, hidden = piece.shape
    return piece.transpose(0, 2, 1, 3).reshape(count, rows, experts * hidden)


def restore_rows(gathered, rows):
    parts = lax.axis_size("tp")
    count, total, width = gathered.shape
    blocks = total // (parts * rows)
    ordered = gathered.reshape(count, parts, blocks, rows, width).transpose(0, 2, 1, 3, 4)
    return ordered.reshape(count, total, width)


def activations(normed, gate_local, up_local, column_weight):
    width = normed.shape[1]
    gate_act = jnp.dot(normed, gate_local, preferred_element_type=jnp.float32) * width ** (-0.5)
    up_act = jnp.dot(normed, up_local, preferred_element_type=jnp.float32) * width ** (-0.5)
    return (column_weight * jax.nn.silu(gate_act) * up_act).astype(jnp.bfloat16)


def route_columns(weight, columns, experts):
    first = lax.axis_index("fs") * columns
    owner = (first + jnp.arange(columns, dtype=jnp.int32)) // FF
    onehot = (owner[None, :] == jnp.arange(experts, dtype=jnp.int32)[:, None]).astype(jnp.float32)
    return jnp.dot(weight, onehot, precision=lax.Precision.HIGHEST)


def shards(
    prompt, norm_gain, gate_master, up_master, down_master, group_choice, inner_choice, route_weight
):
    experts = GROUPS * EPG
    scale = norm_gain[None, :, None]
    gate_cast = (gate_master * scale).astype(jnp.bfloat16)
    up_cast = (up_master * scale).astype(jnp.bfloat16)
    down_cast = down_master.astype(jnp.bfloat16)
    rows = gate_master.shape[1] // lax.axis_size("tp")
    values = prompt.astype(jnp.float32)
    normed = (values * lax.rsqrt(jnp.mean(values * values, axis=1, keepdims=True) + 1e-06)).astype(
        jnp.bfloat16
    )
    chosen = group_choice[:, None] * EPG + inner_choice
    member = (chosen[:, :, None] == jnp.arange(experts, dtype=jnp.int32)[None, None, :]).astype(
        jnp.float32
    )
    weight = jnp.sum(member * route_weight[:, :, None], axis=1)
    stacked = jnp.stack([gate_cast, up_cast, down_cast])
    widened = lax.all_to_all(stacked, "tp", split_axis=2, concat_axis=3, tiled=True)
    moved = lax.all_to_all(flatten_rows(widened), "fs", split_axis=2, concat_axis=1, tiled=True)
    served = restore_rows(lax.all_gather(moved, "tp", axis=1, tiled=True), rows)
    gate_local, up_local, down_local = (served[0], served[1], served[2])
    column_weight = route_columns(weight, gate_local.shape[1], experts)
    scaled = activations(normed, gate_local, up_local, column_weight)
    summed = lax.psum_scatter(
        lax.dot_general(
            down_local, scaled, (((1,), (1,)), ((), ())), preferred_element_type=jnp.float32
        ),
        "fs",
        scatter_dimension=0,
        tiled=True,
    )
    mixed = (summed * FF ** (-0.5)).T.astype(jnp.bfloat16)
    return (gate_local, up_local, down_local, mixed)


def solution(mesh):
    in_specs = (
        P("tp", None),
        P("fs"),
        P(None, "fs", "tp"),
        P(None, "fs", "tp"),
        P(None, "fs", "tp"),
        P("tp"),
        P("tp", None),
        P("tp", None),
    )
    out_specs = (P(None, "fs"), P(None, "fs"), P(None, "fs"), P("tp", "fs"))
    return jax.shard_map(shards, mesh=mesh, in_specs=in_specs, out_specs=out_specs, check_vma=False)
```

profile of v0, /device:TPU:0, one launch (start us, length us, event | category | flops | bytes accessed | tf_op | source)
XLA Modules:
  0.0 666.3 jit_solution(537520447581431105)
XLA Ops:
  7.2 0.0 copy-start.4
  7.2 0.0 all-gather.2.cloned.1.call-start
  7.2 0.0 copy-start
  7.2 4.8 copy.90
  12.0 0.0 copy-done.4
  12.0 0.0 copy-done
  12.0 9.9 %fusion.6 = (bf16[1,32,256,128]{3,1,0,2:T(8,128)(2,1)S(1)}, bf16[1,32,256,128]{3,1,0,2:T(8,128)(2,1)S(1)}) fusion(f32[32,256,128]{2,1,0:T(8,128)S(1)} %copy-done, f32[256]{0:T(256)S(1)} %copy-done.4, f32[32,256,128]{2,1,0:T(8,128)} %param.11), kind=kLoop, calls=%fused_computation.16 | loop fusion | flops 4194304 | bytes 12583936 | tf_op jit(solution)/shard_map/stack | solution.py:56
  22.0 0.8 pad_maximum_fusion
  22.7 75.3 %all_to_all.36 = bf16[3,32,256,128]{3,1,0,2:T(8,128)(2,1)S(1)} all-to-all(bf16[3,32,256,128]{3,1,0,2:T(8,128)(2,1)S(1)} %pad_maximum_fusion), channel_id=1, replica_groups=mesh['fs'=8,'tp'=4] {'tp'}, dimensions={2} | all-to-all | bytes 12582912 | tf_op jit(solution)/shard_map/all_to_all | solution.py:57
  98.0 7.6 %copy.89 = bf16[3,32,4,64,128]{4,2,3,1,0:T(4,128)(2,1)} copy(bf16[3,32,4,64,128]{4,1,0,3,2:T(8,128)(2,1)S(1)} %bitcast.37) | data formatting | bytes 12582912 | tf_op jit(solution)/shard_map/all_to_all | solution.py:57
  105.6 10.1 %all_to_all.29 = bf16[3,32,64,512]{3,2,1,0:T(8,128)(2,1)} reshape(bf16[3,32,64,4,128]{4,3,2,1,0:T(4,128)(2,1)} %bitcast.38) | data formatting | bytes 12582912 | tf_op jit(solution)/shard_map/all_to_all | solution.py:57
  115.7 22.5 %copy.71 = bf16[3,64,32,512]{1,0,3,2:T(4,128)(2,1)} copy(bf16[3,64,32,512]{3,1,2,0:T(8,128)(2,1)} %bitcast.40) | data formatting | bytes 12582912 | tf_op jit(solution)/shard_map/reshape | solution.py:13
  138.3 15.3 %reshape.55 = bf16[8,2,196608]{2,1,0:T(2,128)(2,1)} reshape(bf16[16384,3,64]{2,1,0:T(4,128)(2,1)} %bitcast.34) | data formatting | bytes 12582912
  153.6 144.3 %all_to_all.37 = bf16[8,2,196608]{2,1,0:T(2,128)(2,1)} all-to-all(bf16[8,2,196608]{2,1,0:T(2,128)(2,1)} %reshape.55), channel_id=1, replica_groups=mesh['fs'=8,'tp'=4] {'fs'}, dimensions={0} | all-to-all | bytes 12582912 | tf_op jit(solution)/shard_map/all_to_all | solution.py:58
  297.8 14.2 %reshape.56 = bf16[16384,3,64]{2,1,0:T(4,128)(2,1)} reshape(bf16[8,2,196608]{2,1,0:T(2,128)(2,1)} %all_to_all.37) | data formatting | bytes 12582912
  312.0 23.2 %copy.73 = bf16[3,64,8,2048]{3,1,2,0:T(8,128)(2,1)} copy(bf16[3,64,8,2048]{1,0,3,2:T(4,128)(2,1)} %bitcast.35) | data formatting | bytes 12582912 | tf_op jit(solution)/shard_map/all_to_all | solution.py:58
  335.3 0.0 copy-start.5
  335.3 0.0 copy-start.3
  335.3 0.0 copy-start.2
  335.3 0.0 copy-start.1
  335.3 0.0 all-gather.2.cloned.1.call-update
  335.3 0.3 reduce-scatter.2.cloned.1.call-start
  335.6 0.3 copy-done.5
  336.0 0.0 copy-done.3
  336.0 0.0 copy-done.2
  336.0 0.5 copy-done.1
  336.5 0.3 fusion.4
  336.8 223.6 %all-gather.2.cloned.1.call-done = bf16[3,2048,2048]{2,1,0:T(8,128)(2,1)} async-done(((bf16[3,512,2048]{2,1,0:T(8,128)(2,1)}), bf16[3,2048,2048]{2,1,0:T(8,128)(2,1)}) %all-gather.2.cloned.1.call-update) | async-done | bytes 25165840 | tf_op jit(solution)/shard_map/all_gather | solution.py:59
  560.4 16.8 %fusion.20 = (bf16[1,8,4,64,2048]{4,3,1,2,0:T(8,128)(2,1)}, bf16[1,8,4,64,2048]{4,3,1,2,0:T(8,128)(2,1)}, bf16[1,8,4,64,2048]{4,3,1,2,0:T(8,128)(2,1)}) fusion(bf16[3,8,4,64,2048]{4,3,1,2,0:T(8,128)(2,1)} %bitcast.36), kind=kLoop, calls=%fused_computation.39 | loop fusion | bytes 50331648 | tf_op jit(solution)/shard_map/slice | solution.py:60
  577.2 8.4 %copy.67 = bf16[1,8,4,64,2048]{4,3,2,1,0:T(8,128)(2,1)} copy(bf16[1,8,4,64,2048]{4,3,1,2,0:T(8,128)(2,1)} %get-tuple-element.30) | data formatting | bytes 16777216 | tf_op jit(solution)/shard_map/slice | solution.py:60
  585.7 8.4 %copy.68 = bf16[1,8,4,64,2048]{4,3,2,1,0:T(8,128)(2,1)} copy(bf16[1,8,4,64,2048]{4,3,1,2,0:T(8,128)(2,1)} %get-tuple-element.29) | data formatting | bytes 16777216 | tf_op jit(solution)/shard_map/slice | solution.py:60
  594.1 8.4 %copy.69 = bf16[1,8,4,64,2048]{4,3,2,1,0:T(8,128)(2,1)} copy(bf16[1,8,4,64,2048]{4,3,1,2,0:T(8,128)(2,1)} %get-tuple-element.28) | data formatting | bytes 16777216 | tf_op jit(solution)/shard_map/slice | solution.py:60
  602.5 5.8 convolution_multiply_fusion.1
  608.3 1.4 convolution_multiply_fusion.2
  609.7 11.8 %fusion.14 = f32[2048,256]{1,0:T(8,128)} fusion(bf16[2048,2048]{1,0:T(8,128)(2,1)} %bitcast.45, f32[256,2048]{1,0:T(8,128)S(1)} %convolution_multiply_fusion.2, bf16[2048,2048]{1,0:T(8,128)(2,1)} %bitcast.43, bf16[256,2048]{1,0:T(8,128)(2,1)S(1)} %copy-done.1, f32[256]{0:T(256)S(1)} %add_rsqrt_fusion), kind=kOutput, calls=%fused_computation.23 | convolution fusion | flops 4298113024 | bytes 22021120 | tf_op jit(solution)/shard_map/dot_general | solution.py:64
  621.5 0.0 reduce-scatter.2.cloned.1.call-update
  621.5 36.2 %reduce-scatter.2.cloned.1.call-done = f32[256,256]{1,0:T(8,128)} async-done(((f32[2048,256]{1,0:T(8,128)}), f32[256,256]{1,0:T(8,128)}) %reduce-scatter.2.cloned.1.call-update) | async-done | bytes 262160 | tf_op jit(solution)/shard_map/reduce_scatter | solution.py:63
  657.7 1.0 fusion.11
  658.7 0.8 copy.70
  (5 shorter events, 0.0 us)
Async XLA Ops:
  7.2 4.8 copy-start.4
  7.2 553.3 %all-gather.2.cloned.1.call-start = ((), (), s32[]{:S(2)}) async-start(), calls=%async_computation.3 | async-start | bytes 31457280 | tf_op jit(solution)/shard_map/all_gather | solution.py:59
  7.2 4.8 copy-start
  335.3 0.7 copy-start.5
  335.3 0.7 copy-start.3
  335.3 0.7 copy-start.2
  335.3 1.3 copy-start.1
  335.3 322.4 %reduce-scatter.2.cloned.1.call-start = ((), (), s32[]{:S(2)}) async-start(), calls=%async_computation.4 | async-start | bytes 2359296 | tf_op jit(solution)/shard_map/reduce_scatter | solution.py:63
Sparse Core Ops, SparseCore 0:
  335.4 224.9 all-gather.1
  621.7 35.9 reduce-scatter.1
where the time goes:
time: 669 us; the launch traced here: 666 us
  waiting for transfers between devices  260 us (39%)
  blocking collectives  220 us (33%)
  local copies, waits for them, and re-layouts  142 us (21%)
  matrix products  19 us (3%)
  between operations  14.1 us (2%)
  other arithmetic  12 us (2%)
    all_gather x1, waiting for transfers between devices, shards(): served = restore_rows(lax.all_gather(moved, 'tp', axis=1, tiled=True), rows)  224 us
    all_to_all x1, blocking collectives, shards(): lax.all_to_all(flatten_rows(widened), 'fs', split_axis=2, concat_axis=1,...  144 us
    all_to_all x1, blocking collectives, shards(): lax.all_to_all(stacked, 'tp', split_axis=2, concat_axis=3, tiled=True)  75.3 us
    slice x4, local copies, waits for them, and re-layouts, shards(): gate_local, up_local, down_local = (served[0], served[1], served[2])  42.1 us
    reduce_scatter x1, waiting for transfers between devices, shards(): lax.psum_scatter(lax.dot_general(down_local, scaled, (((1,), (1,)), ((),...  36.2 us
    unnamed x16, local copies, waits for them, and re-layouts  36 us
    all_to_all x1, local copies, waits for them, and re-layouts, shards(): lax.all_to_all(flatten_rows(widened), 'fs', split_axis=2, concat_axis=1,...  23.2 us
    reshape x1, local copies, waits for them, and re-layouts, flatten_rows(): return piece.transpose(0, 2, 1, 3).reshape(count, rows, experts * hidden)  22.5 us
  transfers between devices with their start and end apart: 2, of which 2 were waited for; matrix products, arithmetic and copies ran while one was open for 0% of the time, Pallas kernels for 0%

commit v1 on v0

--- a/solution.py
+++ b/solution.py
@@ -55,7 +55,12 @@
     weight = jnp.sum(member * route_weight[:, :, None], axis=1)
     stacked = jnp.stack([gate_cast, up_cast, down_cast])
     widened = lax.all_to_all(stacked, "tp", split_axis=2, concat_axis=3, tiled=True)
-    moved = lax.all_to_all(flatten_rows(widened), "fs", split_axis=2, concat_axis=1, tiled=True)
+    moved = jnp.concatenate(
+        lax.all_to_all(
+            jnp.stack(jnp.split(flatten_rows(widened), lax.axis_size("fs"), axis=2)), "fs", 0, 0
+        ),
+        axis=1,
+    )
     served = restore_rows(lax.all_gather(moved, "tp", axis=1, tiled=True), rows)
     gate_local, up_local, down_local = (served[0], served[1], served[2])
     column_weight = route_columns(weight, gate_local.shape[1], experts)

time: 669 us -> 598 us (0.89)
  local copies, waits for them, and re-layouts: 142 us -> 73.5 us
    unnamed x16 -> x21, local copies, waits for them, and re-layouts: 36 us -> 6.84 us
    all_to_all x1 -> x0, local copies, waits for them, and re-layouts: 23.2 us -> none  [shards(): lax.all_to_all(flatten_rows(widened), 'fs', split_axis=2, concat_axis=1,...]
    reshape x1, local copies, waits for them, and re-layouts: 22.5 us -> 3.6 us  [flatten_rows(): return piece.transpose(0, 2, 1, 3).reshape(count, rows, experts * hidden)]
where the time goes in v1:
time: 598 us
  waiting for transfers between devices  260 us (43%)
  blocking collectives  219 us (37%)
  local copies, waits for them, and re-layouts  73.5 us (12%)
  matrix products  19 us (3%)
  between operations  14.2 us (2%)
  other arithmetic  12 us (2%)
    all_gather x1, waiting for transfers between devices, shards(): served = restore_rows(lax.all_gather(moved, 'tp', axis=1, tiled=True), rows)  224 us
    all_to_all x1, blocking collectives, shards(): lax.all_to_all(jnp.stack(jnp.split(flatten_rows(widened), lax.axis_size('...  144 us
    all_to_all x1, blocking collectives, shards(): lax.all_to_all(stacked, 'tp', split_axis=2, concat_axis=3, tiled=True)  75.3 us
    slice x4, local copies, waits for them, and re-layouts, shards(): gate_local, up_local, down_local = (served[0], served[1], served[2])  42.1 us
    reduce_scatter x1, waiting for transfers between devices, shards(): lax.psum_scatter(lax.dot_general(down_local, scaled, (((1,), (1,)), ((),...  36.1 us
    all_to_all x2, local copies, waits for them, and re-layouts, shards(): lax.all_to_all(stacked, 'tp', split_axis=2, concat_axis=3, tiled=True)  17.7 us
  transfers between devices with their start and end apart: 2, of which 2 were waited for; matrix products, arithmetic and copies ran while one was open for 0% of the time, Pallas kernels for 0%

profile of v1, /device:TPU:0, one launch (start us, length us, event | category | flops | bytes accessed | tf_op | source)
XLA Modules:
  0.0 597.6 jit_solution(17658314490734537751)
XLA Ops:
  7.2 0.0 copy-start.4
  7.2 0.0 all-gather.2.cloned.1.call-start
  7.2 0.0 copy-start
  7.2 4.8 copy.70
  12.0 0.0 copy-done.4
  12.0 0.0 copy-done
  12.0 9.9 %fusion.6 = (bf16[1,32,256,128]{3,1,0,2:T(8,128)(2,1)S(1)}, bf16[1,32,256,128]{3,1,0,2:T(8,128)(2,1)S(1)}) fusion(f32[32,256,128]{2,1,0:T(8,128)S(1)} %copy-done, f32[256]{0:T(256)S(1)} %copy-done.4, f32[32,256,128]{2,1,0:T(8,128)} %param.11), kind=kLoop, calls=%fused_computation.16 | loop fusion | flops 4194304 | bytes 12583936 | tf_op jit(solution)/shard_map/stack | solution.py:56
  22.0 0.8 pad_maximum_fusion
  22.7 75.3 %all_to_all.23 = bf16[3,32,256,128]{3,1,0,2:T(8,128)(2,1)S(1)} all-to-all(bf16[3,32,256,128]{3,1,0,2:T(8,128)(2,1)S(1)} %pad_maximum_fusion), channel_id=1, replica_groups=mesh['fs'=8,'tp'=4] {'tp'}, dimensions={2} | all-to-all | bytes 12582912 | tf_op jit(solution)/shard_map/all_to_all | solution.py:57
  98.0 7.6 %copy.69 = bf16[3,32,4,64,128]{4,2,3,1,0:T(4,128)(2,1)} copy(bf16[3,32,4,64,128]{4,1,0,3,2:T(8,128)(2,1)S(1)} %bitcast.72) | data formatting | bytes 12582912 | tf_op jit(solution)/shard_map/all_to_all | solution.py:57
  105.6 10.1 %all_to_all.19 = bf16[3,32,64,512]{3,2,1,0:T(8,128)(2,1)} reshape(bf16[3,32,64,4,128]{4,3,2,1,0:T(4,128)(2,1)} %bitcast.73) | data formatting | bytes 12582912 | tf_op jit(solution)/shard_map/all_to_all | solution.py:57
  115.7 3.6 copy.54
  119.3 0.1 fusion.16
  119.4 0.1 fusion.15
  119.4 0.1 fusion.14
  119.5 0.1 fusion.13
  119.6 0.1 fusion.12
  119.6 0.1 fusion.11
  119.7 0.1 fusion.10
  119.7 0.1 fusion.9
  119.8 143.6 %all_to_all.24 = bf16[8,3,64,2048]{3,2,1,0:T(8,128)(2,1)S(1)} all-to-all(bf16[8,3,64,2048]{3,2,1,0:T(8,128)(2,1)S(1)} %fusion.9), channel_id=1, replica_groups=mesh['fs'=8,'tp'=4] {'fs'}, dimensions={0} | all-to-all | bytes 12582912 | tf_op jit(solution)/shard_map/all_to_all | solution.py:59
  263.4 3.3 copy.49
  266.7 0.0 copy-start.5
  266.7 0.0 copy-start.3
  266.7 0.0 copy-start.2
  266.7 0.0 copy-start.1
  266.7 0.0 all-gather.2.cloned.1.call-update
  266.7 0.3 reduce-scatter.2.cloned.1.call-start
  267.0 0.3 copy-done.5
  267.4 0.0 copy-done.3
  267.4 0.0 copy-done.2
  267.4 0.5 copy-done.1
  268.0 0.3 fusion.4
  268.2 223.6 %all-gather.2.cloned.1.call-done = bf16[3,2048,2048]{2,1,0:T(8,128)(2,1)} async-done(((bf16[3,512,2048]{2,1,0:T(8,128)(2,1)}), bf16[3,2048,2048]{2,1,0:T(8,128)(2,1)}) %all-gather.2.cloned.1.call-update) | async-done | bytes 25165840 | tf_op jit(solution)/shard_map/all_gather | solution.py:64
  491.9 16.8 %fusion.28 = (bf16[1,8,4,64,2048]{4,3,1,2,0:T(8,128)(2,1)}, bf16[1,8,4,64,2048]{4,3,1,2,0:T(8,128)(2,1)}, bf16[1,8,4,64,2048]{4,3,1,2,0:T(8,128)(2,1)}) fusion(bf16[3,8,4,64,2048]{4,3,1,2,0:T(8,128)(2,1)} %bitcast.62), kind=kLoop, calls=%fused_computation.55 | loop fusion | bytes 50331648 | tf_op jit(solution)/shard_map/slice | solution.py:65
  508.6 8.4 %copy.50 = bf16[1,8,4,64,2048]{4,3,2,1,0:T(8,128)(2,1)} copy(bf16[1,8,4,64,2048]{4,3,1,2,0:T(8,128)(2,1)} %get-tuple-element.26) | data formatting | bytes 16777216 | tf_op jit(solution)/shard_map/slice | solution.py:65
  517.1 8.4 %copy.51 = bf16[1,8,4,64,2048]{4,3,2,1,0:T(8,128)(2,1)} copy(bf16[1,8,4,64,2048]{4,3,1,2,0:T(8,128)(2,1)} %get-tuple-element.25) | data formatting | bytes 16777216 | tf_op jit(solution)/shard_map/slice | solution.py:65
  525.5 8.4 %copy.52 = bf16[1,8,4,64,2048]{4,3,2,1,0:T(8,128)(2,1)} copy(bf16[1,8,4,64,2048]{4,3,1,2,0:T(8,128)(2,1)} %get-tuple-element.24) | data formatting | bytes 16777216 | tf_op jit(solution)/shard_map/slice | solution.py:65
  534.0 5.8 convolution_multiply_fusion.1
  539.7 1.4 convolution_multiply_fusion.2
  541.1 11.8 %fusion.22 = f32[2048,256]{1,0:T(8,128)} fusion(bf16[2048,2048]{1,0:T(8,128)(2,1)} %bitcast.80, f32[256,2048]{1,0:T(8,128)S(1)} %convolution_multiply_fusion.2, bf16[2048,2048]{1,0:T(8,128)(2,1)} %bitcast.78, bf16[256,2048]{1,0:T(8,128)(2,1)S(1)} %copy-done.1, f32[256]{0:T(256)S(1)} %add_rsqrt_fusion), kind=kOutput, calls=%fused_computation.39 | convolution fusion | flops 4298113024 | bytes 22021120 | tf_op jit(solution)/shard_map/dot_general | solution.py:69
  552.9 0.0 reduce-scatter.2.cloned.1.call-update
  553.0 36.1 %reduce-scatter.2.cloned.1.call-done = f32[256,256]{1,0:T(8,128)} async-done(((f32[2048,256]{1,0:T(8,128)}), f32[256,256]{1,0:T(8,128)}) %reduce-scatter.2.cloned.1.call-update) | async-done | bytes 262160 | tf_op jit(solution)/shard_map/reduce_scatter | solution.py:68
  589.1 1.0 fusion.19
  590.0 0.8 copy.53
  (5 shorter events, 0.0 us)
Async XLA Ops:
  7.2 4.8 copy-start.4
  7.2 484.7 %all-gather.2.cloned.1.call-start = ((), (), s32[]{:S(2)}) async-start(), calls=%async_computation.3 | async-start | bytes 31457280 | tf_op jit(solution)/shard_map/all_gather | solution.py:64
  7.2 4.8 copy-start
  266.7 0.7 copy-start.5
  266.7 0.7 copy-start.3
  266.7 0.7 copy-start.2
  266.7 1.3 copy-start.1
  266.7 322.3 %reduce-scatter.2.cloned.1.call-start = ((), (), s32[]{:S(2)}) async-start(), calls=%async_computation.4 | async-start | bytes 2359296 | tf_op jit(solution)/shard_map/reduce_scatter | solution.py:68
Sparse Core Ops, SparseCore 0:
  266.8 224.9 all-gather.1
  553.1 35.9 reduce-scatter.1
